TPU v7x, 32 devices: a whole 2x2x4 slice. The times are simulated.
32 devices in a mesh: kv: 16 (over z, y, x), tp: 2 (over core).
Axes of the slice: x: 2, y: 2, z: 4, core: 2. Of those that a mesh axis runs over, the one named last changes fastest.
Arguments:
- tokens: bfloat16 [256, 2048], P('kv', 'tp'), may hold values from -20 to 20
- attn_gain: bfloat16 [2048], replicated, may hold values from 0.099609375 to 1.8984375
- query_weight: bfloat16 [2048, 1024], P(None, 'tp'), may hold values from -0.125 to 0.125
- key_weight: bfloat16 [2048, 1024], P(None, 'tp'), may hold values from -0.125 to 0.125
- value_weight: bfloat16 [2048, 1024], P(None, 'tp'), may hold values from -0.125 to 0.125
- outgate_weight: bfloat16 [2048, 1024], P(None, 'tp'), may hold values from -0.125 to 0.125
- gate_weight: bfloat16 [2, 8, 2048], replicated, may hold values from -0.125 to 0.125
- forget_bias: float32 [8], replicated, may hold values from -1 to 4
- state_matrix: float32 [256, 8, 128, 128], P('kv', 'tp'), may hold values from -1.8 to 1.8
- state_norm: float32 [256, 8, 128], P('kv', 'tp'), may hold values from -1.8 to 1.8
- state_max: float32 [256, 8], P('kv', 'tp'), may hold values from -1 to 1
- out_weight: bfloat16 [1024, 2048], P(None, 'tp'), may hold values from -0.1875 to 0.1875
- mlp_gain: bfloat16 [2048], P('tp'), may hold values from 0.099609375 to 1.8984375
- up_weight: bfloat16 [2048, 8192], P('tp', 'kv'), may hold values from -0.125 to 0.125
- down_weight: bfloat16 [8192, 2048], P('kv', 'tp'), may hold values from -0.0625 to 0.0625
Outputs:
- result: bfloat16 [256, 2048], P('kv', 'tp')
- next_matrix: float32 [256, 8, 128, 128], P('kv', 'tp')
- next_norm: float32 [256, 8, 128], P('kv', 'tp')
- next_max: float32 [256, 8], P('kv', 'tp')
All inputs are finite; a program needn't handle non-finite values.
Results may differ from a plain program's by a relative error of at most 0.013.
Values may be sent and summed in bfloat16 or wider, within the bound.
A program may use at most 64 MiB of HBM per device.

v0:
```python
import jax
import jax.numpy as jnp
from jax import lax
from jax.sharding import PartitionSpec as P

epsilon = 1e-06


def body(
    tokens,
    attn_gain,
    query_weight,
    key_weight,
    value_weight,
    outgate_weight,
    gate_weight,
    forget_bias,
    state_matrix,
    state_norm,
    state_max,
    out_weight,
    mlp_gain,
    up_weight,
    down_weight,
):
    sequences = tokens.shape[0]
    local_heads = state_matrix.shape[1]
    head_dim = state_matrix.shape[2]
    width = query_weight.shape[1]
    model_width = attn_gain.shape[0]
    first_head = lax.axis_index("tp") * local_heads
    my_gates = lax.dynamic_slice_in_dim(gate_weight, first_head, local_heads, 1).reshape(
        2 * local_heads, model_width
    )
    my_bias = lax.dynamic_slice_in_dim(forget_bias, first_head, local_heads, 0)
    gain_full = attn_gain.astype(jnp.float32)
    seg_values = lax.all_gather(tokens, "tp", axis=1, tiled=True).astype(jnp.float32)
    scaled = (seg_values * gain_full).astype(jnp.bfloat16)

    def product(weight):
        return jnp.dot(scaled, weight, preferred_element_type=jnp.float32)

    gate_part = jnp.einsum("sd,gd->sg", scaled, my_gates, preferred_element_type=jnp.float32)
    squares = jnp.sum(seg_values * seg_values, axis=1)
    query_acc = product(query_weight)
    key_acc = product(key_weight)
    value_acc = product(value_weight)
    outgate_acc = product(outgate_weight)
    scale_in = lax.rsqrt(squares / model_width + epsilon)[:, None]
    query_rows = (query_acc * scale_in).reshape(sequences, local_heads, head_dim)
    key_rows = (key_acc * scale_in * head_dim ** (-0.5)).reshape(sequences, local_heads, head_dim)
    value_rows = (value_acc * scale_in).reshape(sequences, local_heads, head_dim)
    outgate = (outgate_acc * scale_in).reshape(sequences, local_heads, head_dim)
    gate_pre = gate_part * scale_in
    in_gate = gate_pre[:, :local_heads]
    forget_log = jax.nn.log_sigmoid(gate_pre[:, local_heads:] + my_bias)
    next_max = jnp.maximum(forget_log + state_max, in_gate)
    kept_share = jnp.exp(forget_log + state_max - next_max)
    admitted = jnp.exp(in_gate - next_max)
    next_matrix = (
        kept_share[:, :, None, None] * state_matrix
        + admitted[:, :, None, None] * key_rows[:, :, :, None] * value_rows[:, :, None, :]
    )
    next_norm = kept_share[:, :, None] * state_norm + admitted[:, :, None] * key_rows
    numerator = jnp.einsum(
        "shd,shde->she", query_rows, next_matrix, precision=lax.Precision.HIGHEST
    )
    denominator = jnp.sum(query_rows * next_norm, axis=2)
    head_out = numerator / jnp.maximum(jnp.abs(denominator), 1.0)[:, :, None]
    mixed = (head_out * jax.nn.sigmoid(outgate)).reshape(sequences, width).astype(jnp.bfloat16)
    attended = jnp.dot(
        lax.all_gather(mixed, "tp", axis=1, tiled=True),
        out_weight,
        preferred_element_type=jnp.float32,
    )
    residual = (tokens.astype(jnp.float32) + attended).astype(jnp.bfloat16)
    gain_mid = mlp_gain.astype(jnp.float32)
    rows_all = lax.all_gather(residual, "kv", axis=0, tiled=True)
    row_values = rows_all.astype(jnp.float32)
    row_squares = jnp.sum(row_values * row_values, axis=1)
    scaled_mid = (row_values * gain_mid).astype(jnp.bfloat16)
    partial_value = jnp.dot(scaled_mid, up_weight, preferred_element_type=jnp.float32)
    summed = lax.psum(partial_value.astype(jnp.bfloat16), "tp").astype(jnp.float32)
    total_squares = lax.psum(row_squares.astype(jnp.bfloat16), "tp").astype(jnp.float32)
    up_value = summed * lax.rsqrt(total_squares / model_width + epsilon)[:, None]
    hidden = jnp.square(jax.nn.relu(up_value)).astype(jnp.bfloat16)
    mixer_out = lax.psum_scatter(
        jnp.dot(hidden, down_weight, preferred_element_type=jnp.float32),
        "kv",
        scatter_dimension=0,
        tiled=True,
    )
    result = (residual.astype(jnp.float32) + mixer_out).astype(jnp.bfloat16)
    return (result, next_matrix, next_norm, next_max)


def solution(mesh):
    in_specs = (
        P("kv", "tp"),
        P(),
        P(None, "tp"),
        P(None, "tp"),
        P(None, "tp"),
        P(None, "tp"),
        P(),
        P(),
        P("kv", "tp", None, None),
        P("kv", "tp", None),
        P("kv", "tp"),
        P(None, "tp"),
        P("tp"),
        P("tp", "kv"),
        P("kv", "tp"),
    )
    out_specs = (P("kv", "tp"), P("kv", "tp", None, None), P("kv", "tp", None), P("kv", "tp"))
    return jax.shard_map(body, mesh=mesh, in_specs=in_specs, out_specs=out_specs, check_vma=False)
```

profile of v0, /device:TPU:0, one launch (start us, length us, event | category | flops | bytes accessed | tf_op | source)
XLA Modules:
  0.0 179.5 jit_solution(18217517377536054853)
XLA Ops:
  7.3 0.8 convert_element_type.53
  8.1 2.2 %all_gather.9 = bf16[16,2048]{1,0:T(8,128)(2,1)S(1)} all-gather(bf16[16,1024]{1,0:T(8,128)(2,1)} %param.15), channel_id=1, replica_groups=mesh['kv'=16,'tp'=2] {'tp'}, dimensions={1}, use_global_device_ids=true | all-gather | bytes 98304 | tf_op jit(solution)/shard_map/all_gather | solution.py:37
  10.3 0.1 fusion.14
  10.4 1.9 %convolution_multiply_fusion.3 = f32[16,512]{1,0:T(8,128)S(1)} fusion(bf16[2048,512]{1,0:T(8,128)(2,1)} %param.17, bf16[16,2048]{1,0:T(8,128)(2,1)S(1)} %all_gather.9, f32[2048]{0:T(1024)S(1)} %convert_element_type.53, f32[16]{0:T(128)S(1)} %add_rsqrt_fusion.1), kind=kOutput, calls=%fused_computation.11 | convolution fusion | flops 33660928 | bytes 2203712 | tf_op jit(solution)/shard_map/dot_general | solution.py:41
  12.6 0.1 convolution_multiply_fusion.4
  12.8 0.1 subtract_exponential_fusion.1
  12.9 0.1 copy.19
  13.1 1.9 %fusion.3 = f32[16,512]{1,0:T(8,128)S(1)} fusion(bf16[2048,512]{1,0:T(8,128)(2,1)} %param.18, bf16[16,2048]{1,0:T(8,128)(2,1)S(1)} %all_gather.9, f32[2048]{0:T(1024)S(1)} %convert_element_type.53, f32[16]{0:T(128)S(1)} %add_rsqrt_fusion.1), kind=kOutput, calls=%fused_computation.12 | convolution fusion | flops 33669120 | bytes 2203712 | tf_op jit(solution)/shard_map/dot_general | solution.py:41
  15.1 0.7 multiply_reduce_fusion
  15.8 1.9 %convolution_multiply_fusion.1 = f32[16,512]{1,0:T(8,128)S(1)} fusion(bf16[2048,512]{1,0:T(8,128)(2,1)} %param.19, bf16[16,2048]{1,0:T(8,128)(2,1)S(1)} %all_gather.9, f32[2048]{0:T(1024)S(1)} %convert_element_type.53, f32[16]{0:T(128)S(1)} %add_rsqrt_fusion.1), kind=kOutput, calls=%fused_computation.9 | convolution fusion | flops 33660928 | bytes 2203712 | tf_op jit(solution)/shard_map/dot_general | solution.py:41
  17.8 0.4 fusion.5
  18.2 3.0 %multiply_add_fusion = f32[16,4,128,128]{3,2,1,0:T(8,128)S(1)} fusion(f32[16,4,128,128]{3,2,1,0:T(8,128)} %param.23, f32[16,4,128]{2,1,0:T(4,128)S(1)} %mul.144, f32[16,4,128]{2,1,0:T(4,128)S(1)} %get-tuple-element.6, f32[16,4]{1,0:T(8,128)S(1)} %copy.19), kind=kLoop, calls=%fused_computation | loop fusion | flops 3145728 | bytes 8454400 | tf_op jit(solution)/shard_map/add | solution.py:61
  21.3 3.7 %fusion.24 = f32[16,4,1,128]{3,2,1,0:T(1,128)S(1)} fusion(f32[16,4,128,1]{2,3,1,0:T(1,128)S(1)} %bitcast.18, f32[16,4,128,128]{3,2,1,0:T(8,128)S(1)} %multiply_add_fusion), kind=kOutput, calls=%fused_computation.45 | convolution fusion | flops 12582912 | bytes 4259840 | tf_op jit(solution)/shard_map/shd,shde->she/dot_general | solution.py:65
  25.0 0.1 fusion.15
  25.1 2.0 %all_gather.10 = bf16[16,1024]{1,0:T(8,128)(2,1)S(1)} all-gather(bf16[16,512]{1,0:T(8,128)(2,1)S(1)} %bitcast.20), channel_id=1, replica_groups=mesh['kv'=16,'tp'=2] {'tp'}, dimensions={1}, use_global_device_ids=true | all-gather | bytes 49152 | tf_op jit(solution)/shard_map/all_gather | solution.py:72
  27.0 0.4 fusion
  27.4 45.4 %all_gather.11 = bf16[256,1024]{1,0:T(8,128)(2,1)S(1)} all-gather(bf16[16,1024]{1,0:T(8,128)(2,1)S(1)} %fusion), channel_id=1, replica_groups=mesh['kv'=16,'tp'=2] {'kv'}, dimensions={0}, use_global_device_ids=true | all-gather | bytes 557056 | tf_op jit(solution)/shard_map/all_gather | solution.py:78
  72.8 1.2 convolution_convert_fusion
  74.1 0.2 fusion.7
  74.2 2.5 %psum.15 = bf16[256]{0:T(256)(128)(2,1)S(1)} all-reduce(bf16[256]{0:T(256)(128)(2,1)S(1)} %fusion.7), channel_id=1, replica_groups=mesh['kv'=16,'tp'=2] {'tp'}, use_global_device_ids=true, to_apply=%region_4.5 | all-reduce | flops 256 | bytes 1024 | tf_op jit(solution)/shard_map/psum | solution.py:84
  76.7 11.5 %all-reduce.2.cloned.1.call-done = bf16[256,512]{1,0:T(8,128)(2,1)} async-done(((bf16[256,512]{1,0:T(8,128)(2,1)}), bf16[256,512]{1,0:T(8,128)(2,1)}) %all-reduce.2.cloned.1.call-update) | async-done | bytes 262160 | tf_op jit(solution)/shard_map/psum | solution.py:83
  88.3 2.8 %fusion.10 = f32[256,1024]{1,0:T(8,128)} fusion(bf16[512,1024]{1,0:T(8,128)(2,1)} %param.29, bf16[256,512]{1,0:T(8,128)(2,1)} %all-reduce.2.cloned.1.call-done, f32[256]{0:T(256)S(1)} %add_rsqrt_fusion), kind=kOutput, calls=%fused_computation.20 | convolution fusion | flops 269090816 | bytes 2360320 | tf_op jit(solution)/shard_map/dot_general | solution.py:88
  91.1 80.1 %reduce-scatter.2.cloned.1.call-done = f32[16,1024]{1,0:T(8,128)} async-done(((f32[256,1024]{1,0:T(8,128)}), f32[16,1024]{1,0:T(8,128)}) %reduce-scatter.2.cloned.1.call-update) | async-done | bytes 65552 | tf_op jit(solution)/shard_map/reduce_scatter | solution.py:87
  171.2 1.5 add_convert_fusion
  (41 shorter events, 0.6 us)
Async XLA Ops:
  7.2 19.9 %copy-start = (bf16[1024,1024]{1,0:T(8,128)(2,1)S(1)}, bf16[1024,1024]{1,0:T(8,128)(2,1)}, u32[]{:S(2)}) copy-start(bf16[1024,1024]{1,0:T(8,128)(2,1)} %param.26) | copy-start | bytes 6291460
  7.2 5.3 %copy-start.7 = (bf16[1024]{0:T(1024)(128)(2,1)S(1)}, bf16[1024]{0:T(1024)(128)(2,1)}, u32[]{:S(2)}) copy-start(bf16[1024]{0:T(1024)(128)(2,1)} %param.27) | copy-start | bytes 6148
  7.2 5.3 %copy-start.10 = (f32[8]{0:T(128)S(1)}, f32[8]{0:T(128)}, u32[]{:S(2)}) copy-start(f32[8]{0:T(128)} %param.22) | copy-start | bytes 100
  7.2 5.4 %copy-start.5 = (bf16[2,8,2048]{2,1,0:T(8,128)(2,1)S(1)}, bf16[2,8,2048]{2,1,0:T(8,128)(2,1)}, u32[]{:S(2)}) copy-start(bf16[2,8,2048]{2,1,0:T(8,128)(2,1)} %param.21) | copy-start | bytes 196612
  7.2 5.6 %copy-start.8 = (f32[16,4]{0,1:T(4,128)S(1)}, f32[16,4]{0,1:T(4,128)}, u32[]{:S(2)}) copy-start(f32[16,4]{0,1:T(4,128)} %param.25) | copy-start | bytes 772
  7.2 81.0 %all-reduce.2.cloned.1.call-start = ((), (), s32[]{:S(2)}) async-start(), calls=%async_computation.1 | async-start | bytes 524288 | tf_op jit(solution)/shard_map/psum | solution.py:83
  10.4 4.6 %copy-start.4 = (f32[16,4,128]{2,1,0:T(4,128)S(1)}, f32[16,4,128]{2,1,0:T(4,128)}, u32[]{:S(2)}) copy-start(f32[16,4,128]{2,1,0:T(4,128)} %param.24) | copy-start | bytes 98308
  12.9 4.9 %copy-start.6 = (f32[16,4]{0,1:T(4,128)}, f32[16,4]{0,1:T(4,128)S(1)}, u32[]{:S(2)}) copy-start(f32[16,4]{0,1:T(4,128)S(1)} %get-tuple-element.8) | copy-start | bytes 772
  15.1 2.7 %copy-start.2 = (bf16[2048,512]{1,0:T(8,128)(2,1)S(1)}, bf16[2048,512]{1,0:T(8,128)(2,1)}, u32[]{:S(2)}) copy-start(bf16[2048,512]{1,0:T(8,128)(2,1)} %param.20) | copy-start | bytes 6291460
  21.3 3.7 %copy-start.1 = (f32[16,4,128,128]{3,2,1,0:T(8,128)}, f32[16,4,128,128]{3,2,1,0:T(8,128)S(1)}, u32[]{:S(2)}) copy-start(f32[16,4,128,128]{3,2,1,0:T(8,128)S(1)} %multiply_add_fusion) | copy-start | bytes 12582916
  21.3 5.8 %copy-start.3 = (bf16[16,1024]{1,0:T(8,128)(2,1)S(1)}, bf16[16,1024]{1,0:T(8,128)(2,1)}, u32[]{:S(2)}) copy-start(bf16[16,1024]{1,0:T(8,128)(2,1)} %param.15) | copy-start | bytes 98308
  25.0 47.9 %copy-start.9 = (bf16[1024,512]{1,0:T(8,128)(2,1)S(1)}, bf16[1024,512]{1,0:T(8,128)(2,1)}, u32[]{:S(2)}) copy-start(bf16[1024,512]{1,0:T(8,128)(2,1)} %param.28) | copy-start | bytes 3145732
  74.0 97.2 %reduce-scatter.2.cloned.1.call-start = ((), (), s32[]{:S(2)}) async-start(), calls=%async_computation.2 | async-start | bytes 1114112 | tf_op jit(solution)/shard_map/reduce_scatter | solution.py:87
Sparse Core Ops, SparseCore 0:
  74.1 14.0 all-reduce.1
  91.2 79.9 reduce-scatter.1
where the time goes:
time: 180 us; the launch traced here: 179 us
  waiting for transfers between devices  91.7 us (51%)
  blocking collectives  52 us (29%)
  matrix products  14.3 us (8%)
  between operations  14.3 us (8%)
  other arithmetic  6.56 us (4%)
    reduce_scatter x1, waiting for transfers between devices, body(): lax.psum_scatter(jnp.dot(hidden, down_weight, preferred_element_type=jnp....  80.1 us
    all_gather x1, blocking collectives, body(): rows_all = lax.all_gather(residual, 'kv', axis=0, tiled=True)  45.4 us
    psum x1, waiting for transfers between devices, body(): lax.psum(partial_value.astype(jnp.bfloat16), 'tp').astype(jnp.float32)  11.5 us
    dot_general x4, matrix products, product(): return jnp.dot(scaled, weight, preferred_element_type=jnp.float32)  6.2 us
    dot_general x1, matrix products, body(): jnp.einsum('shd,shde->she', query_rows, next_matrix, precision=lax.Precis...  3.66 us
  transfers between devices with their start and end apart: 2, of which 2 were waited for; matrix products, arithmetic and copies ran while one was open for 0% of the time, Pallas kernels for 0%

commit v1 on v0

--- a/solution.py
+++ b/solution.py
@@ -80,7 +80,8 @@
     row_squares = jnp.sum(row_values * row_values, axis=1)
     scaled_mid = (row_values * gain_mid).astype(jnp.bfloat16)
     partial_value = jnp.dot(scaled_mid, up_weight, preferred_element_type=jnp.float32)
-    summed = lax.psum(partial_value.astype(jnp.bfloat16), "tp").astype(jnp.float32)
+    assign_fields = lambda matrix, axis_name: jnp.sum(jax.lax.all_gather(matrix, axis_name), axis=0)
+    summed = assign_fields(partial_value.astype(jnp.bfloat16), "tp").astype(jnp.float32)
     total_squares = lax.psum(row_squares.astype(jnp.bfloat16), "tp").astype(jnp.float32)
     up_value = summed * lax.rsqrt(total_squares / model_width + epsilon)[:, None]
     hidden = jnp.square(jax.nn.relu(up_value)).astype(jnp.bfloat16)

time: 180 us -> 165 us (0.917)
  waiting for transfers between devices: 91.7 us -> 74.7 us
  blocking collectives: 52 us -> 54.1 us
    psum x1 -> x0, waiting for transfers between devices: 11.5 us -> none  [body(): lax.psum(partial_value.astype(jnp.bfloat16), 'tp').astype(jnp.float32)]
    reduce_scatter x1, waiting for transfers between devices: 80.1 us -> 74.7 us  [body(): lax.psum_scatter(jnp.dot(hidden, down_weight, preferred_element_type=jnp....]
    all_gather x0 -> x1, blocking collectives: none -> 2.18 us  [body(): jax.lax.all_gather(matrix, axis_name)]
  transfers between devices with their start and end apart: 2 -> 1, of which waited for: 2 -> 1; matrix products, arithmetic and copies ran while one was open for 0% -> 0% of each run, Pallas kernels for 0% -> 0%
where the time goes in v1:
time: 165 us
  waiting for transfers between devices  74.7 us (45%)
  blocking collectives  54.1 us (33%)
  matrix products  14.8 us (9%)
  between operations  14.3 us (9%)
  other arithmetic  6.65 us (4%)
    reduce_scatter x1, waiting for transfers between devices, body(): lax.psum_scatter(jnp.dot(hidden, down_weight, preferred_element_type=jnp....  74.7 us
    all_gather x1, blocking collectives, body(): rows_all = lax.all_gather(residual, 'kv', axis=0, tiled=True)  45.4 us
    dot_general x4, matrix products, product(): return jnp.dot(scaled, weight, preferred_element_type=jnp.float32)  6.2 us
    dot_general x1, matrix products, body(): jnp.einsum('shd,shde->she', query_rows, next_matrix, precision=lax.Precis...  3.66 us
  transfers between devices with their start and end apart: 1, of which 1 were waited for; matrix products, arithmetic and copies ran while one was open for 0% of the time, Pallas kernels for 0%

profile of v1, /device:TPU:0, one launch (start us, length us, event | category | flops | bytes accessed | tf_op | source)
XLA Modules:
  0.0 165.1 jit_solution(2728732152902404376)
XLA Ops:
  7.3 0.8 convert_element_type.55
  8.1 2.2 %all_gather.15 = bf16[16,2048]{1,0:T(8,128)(2,1)S(1)} all-gather(bf16[16,1024]{1,0:T(8,128)(2,1)} %param.15), channel_id=1, replica_groups=mesh['kv'=16,'tp'=2] {'tp'}, dimensions={1}, use_global_device_ids=true | all-gather | bytes 98304 | tf_op jit(solution)/shard_map/all_gather | solution.py:37
  10.3 0.1 fusion.14
  10.4 1.9 %convolution_multiply_fusion.3 = f32[16,512]{1,0:T(8,128)S(1)} fusion(bf16[2048,512]{1,0:T(8,128)(2,1)} %param.17, bf16[16,2048]{1,0:T(8,128)(2,1)S(1)} %all_gather.15, f32[2048]{0:T(1024)S(1)} %convert_element_type.55, f32[16]{0:T(128)S(1)} %add_rsqrt_fusion.1), kind=kOutput, calls=%fused_computation.11 | convolution fusion | flops 33660928 | bytes 2203712 | tf_op jit(solution)/shard_map/dot_general | solution.py:41
  12.6 0.1 convolution_multiply_fusion.4
  12.8 0.1 subtract_exponential_fusion.1
  13.1 1.9 %fusion.3 = f32[16,512]{1,0:T(8,128)S(1)} fusion(bf16[2048,512]{1,0:T(8,128)(2,1)} %param.18, bf16[16,2048]{1,0:T(8,128)(2,1)S(1)} %all_gather.15, f32[2048]{0:T(1024)S(1)} %convert_element_type.55, f32[16]{0:T(128)S(1)} %add_rsqrt_fusion.1), kind=kOutput, calls=%fused_computation.12 | convolution fusion | flops 33669120 | bytes 2203712 | tf_op jit(solution)/shard_map/dot_general | solution.py:41
  15.1 0.7 multiply_reduce_fusion
  15.8 1.9 %convolution_multiply_fusion.1 = f32[16,512]{1,0:T(8,128)S(1)} fusion(bf16[2048,512]{1,0:T(8,128)(2,1)} %param.19, bf16[16,2048]{1,0:T(8,128)(2,1)S(1)} %all_gather.15, f32[2048]{0:T(1024)S(1)} %convert_element_type.55, f32[16]{0:T(128)S(1)} %add_rsqrt_fusion.1), kind=kOutput, calls=%fused_computation.9 | convolution fusion | flops 33660928 | bytes 2203712 | tf_op jit(solution)/shard_map/dot_general | solution.py:41
  17.8 0.4 fusion.5
  18.2 3.0 %multiply_add_fusion = f32[16,4,128,128]{3,2,1,0:T(8,128)S(1)} fusion(f32[16,4,128,128]{3,2,1,0:T(8,128)} %param.23, f32[16,4,128]{2,1,0:T(4,128)S(1)} %mul.144, f32[16,4,128]{2,1,0:T(4,128)S(1)} %get-tuple-element.6, f32[16,4]{1,0:T(8,128)S(1)} %copy.19), kind=kLoop, calls=%fused_computation | loop fusion | flops 3145728 | bytes 8454400 | tf_op jit(solution)/shard_map/add | solution.py:61
  21.3 3.7 %fusion.24 = f32[16,4,1,128]{3,2,1,0:T(1,128)S(1)} fusion(f32[16,4,128,1]{2,3,1,0:T(1,128)S(1)} %bitcast.20, f32[16,4,128,128]{3,2,1,0:T(8,128)S(1)} %multiply_add_fusion), kind=kOutput, calls=%fused_computation.45 | convolution fusion | flops 12582912 | bytes 4259840 | tf_op jit(solution)/shard_map/shd,shde->she/dot_general | solution.py:65
  25.0 0.1 fusion.15
  25.1 1.8 %all_gather.16 = bf16[16,1024]{1,0:T(8,128)(2,1)S(1)} all-gather(bf16[16,512]{1,0:T(8,128)(2,1)S(1)} %bitcast.22), channel_id=1, replica_groups=mesh['kv'=16,'tp'=2] {'tp'}, dimensions={1}, use_global_device_ids=true | all-gather | bytes 49152 | tf_op jit(solution)/shard_map/all_gather | solution.py:72
  26.9 0.4 fusion
  27.3 45.4 %all_gather.17 = bf16[256,1024]{1,0:T(8,128)(2,1)S(1)} all-gather(bf16[16,1024]{1,0:T(8,128)(2,1)S(1)} %fusion), channel_id=1, replica_groups=mesh['kv'=16,'tp'=2] {'kv'}, dimensions={0}, use_global_device_ids=true | all-gather | bytes 557056 | tf_op jit(solution)/shard_map/all_gather | solution.py:78
  72.7 0.2 fusion.7
  72.9 2.5 %psum.7 = bf16[256]{0:T(256)(128)(2,1)S(1)} all-reduce(bf16[256]{0:T(256)(128)(2,1)S(1)} %fusion.7), channel_id=1, replica_groups=mesh['kv'=16,'tp'=2] {'tp'}, use_global_device_ids=true, to_apply=%region_4.5 | all-reduce | flops 256 | bytes 1024 | tf_op jit(solution)/shard_map/psum | solution.py:85
  75.3 1.7 %convolution_convert_fusion = bf16[256,512]{1,0:T(8,128)(2,1)S(1)} fusion(bf16[1024,512]{1,0:T(8,128)(2,1)} %param.28, bf16[256,1024]{1,0:T(8,128)(2,1)S(1)} %all_gather.17, f32[1024]{0:T(1024)S(1)} %convert_element_type.62), kind=kOutput, calls=%fused_computation.3 | convolution fusion | flops 269352960 | bytes 1839104 | tf_op jit(solution)/shard_map/dot_general | solution.py:82
  77.0 2.2 %all-gather = bf16[512,512]{1,0:T(8,128)(2,1)S(1)} all-gather(bf16[256,512]{1,0:T(8,128)(2,1)S(1)} %convolution_convert_fusion), channel_id=2, replica_groups=mesh['kv'=16,'tp'=2] {'tp'}, dimensions={0}, use_global_device_ids=true | all-gather | bytes 786432 | tf_op jit(solution)/shard_map/all_gather | solution.py:83
  79.2 0.1 reduce_sum.41
  79.3 2.7 %fusion.10 = f32[256,1024]{1,0:T(8,128)} fusion(bf16[512,1024]{1,0:T(8,128)(2,1)} %param.29, bf16[256,512]{1,0:T(8,128)(2,1)S(1)} %reduce_sum.41, f32[256]{0:T(256)S(1)} %add_rsqrt_fusion), kind=kOutput, calls=%fused_computation.20 | convolution fusion | flops 269090816 | bytes 2360320 | tf_op jit(solution)/shard_map/dot_general | solution.py:89
  82.1 74.7 %reduce-scatter.2.cloned.1.call-done = f32[16,1024]{1,0:T(8,128)} async-done(((f32[256,1024]{1,0:T(8,128)}), f32[16,1024]{1,0:T(8,128)}) %reduce-scatter.2.cloned.1.call-update) | async-done | bytes 65552 | tf_op jit(solution)/shard_map/reduce_scatter | solution.py:88
  156.7 1.5 add_convert_fusion
  (38 shorter events, 0.6 us)
Async XLA Ops:
  7.2 19.7 %copy-start = (bf16[1024,1024]{1,0:T(8,128)(2,1)S(1)}, bf16[1024,1024]{1,0:T(8,128)(2,1)}, u32[]{:S(2)}) copy-start(bf16[1024,1024]{1,0:T(8,128)(2,1)} %param.26) | copy-start | bytes 6291460
  7.2 5.3 %copy-start.7 = (bf16[1024]{0:T(1024)(128)(2,1)S(1)}, bf16[1024]{0:T(1024)(128)(2,1)}, u32[]{:S(2)}) copy-start(bf16[1024]{0:T(1024)(128)(2,1)} %param.27) | copy-start | bytes 6148
  7.2 5.3 %copy-start.9 = (f32[8]{0:T(128)S(1)}, f32[8]{0:T(128)}, u32[]{:S(2)}) copy-start(f32[8]{0:T(128)} %param.22) | copy-start | bytes 100
  7.2 5.4 %copy-start.5 = (bf16[2,8,2048]{2,1,0:T(8,128)(2,1)S(1)}, bf16[2,8,2048]{2,1,0:T(8,128)(2,1)}, u32[]{:S(2)}) copy-start(bf16[2,8,2048]{2,1,0:T(8,128)(2,1)} %param.21) | copy-start | bytes 196612
  7.2 5.6 %copy-start.8 = (f32[16,4]{0,1:T(4,128)S(1)}, f32[16,4]{0,1:T(4,128)}, u32[]{:S(2)}) copy-start(f32[16,4]{0,1:T(4,128)} %param.25) | copy-start | bytes 772
  7.2 149.5 %reduce-scatter.2.cloned.1.call-start = ((), (), s32[]{:S(2)}) async-start(), calls=%async_computation.1 | async-start | bytes 1114112 | tf_op jit(solution)/shard_map/reduce_scatter | solution.py:88
  10.4 4.6 %copy-start.4 = (f32[16,4,128]{2,1,0:T(4,128)S(1)}, f32[16,4,128]{2,1,0:T(4,128)}, u32[]{:S(2)}) copy-start(f32[16,4,128]{2,1,0:T(4,128)} %param.24) | copy-start | bytes 98308
  12.9 4.9 %copy-start.6 = (f32[16,4]{0,1:T(4,128)}, f32[16,4]{0,1:T(4,128)S(1)}, u32[]{:S(2)}) copy-start(f32[16,4]{0,1:T(4,128)S(1)} %get-tuple-element.8) | copy-start | bytes 772
  15.1 2.7 %copy-start.2 = (bf16[2048,512]{1,0:T(8,128)(2,1)S(1)}, bf16[2048,512]{1,0:T(8,128)(2,1)}, u32[]{:S(2)}) copy-start(bf16[2048,512]{1,0:T(8,128)(2,1)} %param.20) | copy-start | bytes 6291460
  21.3 3.7 %copy-start.1 = (f32[16,4,128,128]{3,2,1,0:T(8,128)}, f32[16,4,128,128]{3,2,1,0:T(8,128)S(1)}, u32[]{:S(2)}) copy-start(f32[16,4,128,128]{3,2,1,0:T(8,128)S(1)} %multiply_add_fusion) | copy-start | bytes 12582916
  21.3 5.6 %copy-start.3 = (bf16[16,1024]{1,0:T(8,128)(2,1)S(1)}, bf16[16,1024]{1,0:T(8,128)(2,1)}, u32[]{:S(2)}) copy-start(bf16[16,1024]{1,0:T(8,128)(2,1)} %param.15) | copy-start | bytes 98308
Sparse Core Ops, SparseCore 0:
  82.2 74.5 reduce-scatter.1
